TPU v7x, 32 devices: a whole 2x2x4 slice. The times are simulated.
32 devices in a mesh: ep: 8 (over z, x), tp: 4 (over y, core).
Axes of the slice: x: 2, y: 2, z: 4, core: 2. Of those that a mesh axis runs over, the one named last changes fastest.
Arguments:
- hidden_in: bfloat16 [128, 4096], P('ep'), may hold values from -6 to 6
- w_query: bfloat16 [4096, 2048], P('ep', 'tp'), may hold values from -0.09375 to 0.09375
- w_key: bfloat16 [4096, 2048], P('ep', 'tp'), may hold values from -0.09375 to 0.09375
- w_value: bfloat16 [4096, 2048], P('ep', 'tp'), may hold values from -0.09375 to 0.09375
- w_outgate: bfloat16 [4096, 2048], P('ep', 'tp'), may hold values from -0.09375 to 0.09375
- w_igate: bfloat16 [4096, 16], P('ep', 'tp'), may hold values from -0.09375 to 0.09375
- w_fgate: bfloat16 [4096, 16], P('ep', 'tp'), may hold values from -0.09375 to 0.09375
- input_bias: float32 [16], P('tp'), may hold values from -3 to 303
- forget_bias: float32 [16], P('tp'), may hold values from -1 to 5
- mem_state: float32 [128, 16, 16384], P('ep', 'tp'), may hold values from -4 to 4
- max_state: float32 [128, 16], P('ep', 'tp'), may hold values from -4 to 304
- head_gain: float32 [2048], P('tp'), may hold values from 0.1 to 1.9
- w_output: bfloat16 [2048, 4096], P('tp'), may hold values from -0.26367188 to 0.26367188
- first_gain: float32 [4096], replicated, may hold values from 0.35 to 3.25
- w_group_router: bfloat16 [4096, 2], replicated, may hold values from -0.09375 to 0.09375
- w_expert_router: bfloat16 [4096, 8], replicated, may hold values from -0.09375 to 0.09375
- expert_route: int32 [128, 2], P('ep'), may hold values from 0 to 7, as said below
- w_expgate: bfloat16 [8, 4096, 1024], P('ep', None, 'tp'), may hold values from -0.09375 to 0.09375
- w_expup: bfloat16 [8, 4096, 1024], P('ep', None, 'tp'), may hold values from -0.09375 to 0.09375
- w_expdown: bfloat16 [8, 1024, 4096], P('ep', 'tp'), may hold values from -0.75 to 0.75
- second_gain: float32 [4096], P('tp'), may hold values from 0.1 to 1.9
Outputs:
- hidden_out: bfloat16 [128, 4096], P('ep', 'tp')
- mem_next: float32 [128, 16, 16384], P('ep', 'tp')
- max_next: float32 [128, 16], P('ep', 'tp')
Inputs may be any that keep to these rules, and one draw needn't show every extreme that they name: `expert_route`: each row names two different experts of one group (an expert's group is its number divided by 4). In each aligned block of 16 rows (the rows of one index of ep) every group is named by exactly 8 rows, no expert by more than 8 rows, and some expert by exactly 8 rows.
All inputs are finite; a program needn't handle non-finite values.
Results may differ from a plain program's by a relative error of at most 0.02.
Values may be sent and summed in bfloat16 or wider, within the bound.
A program may use at most 64 MiB of HBM per device.

v0:
```python
import jax
import jax.numpy as jnp
from jax import lax
from jax.sharding import PartitionSpec as P

D = 4096
DH = 128
GROUP_SIZE = 4


res_alpha = 8.0**0.25


def layer_norm(values, gain):
    row_mean = jnp.mean(values, -1, keepdims=True)
    row_var = jnp.mean(values * values, -1, keepdims=True) - row_mean * row_mean
    return (values - row_mean) * lax.rsqrt(row_var + 1e-05) * gain


def mlstm_step(queries, keys_scaled, values, log_input, log_forget, memory, stabilizer):
    new_max = jnp.maximum(log_forget + stabilizer, log_input)
    keep_old = jnp.exp(log_forget + stabilizer - new_max)
    write_new = jnp.exp(log_input - new_max)
    scores = jnp.sum(queries * keys_scaled, -1) * write_new
    read_old = jnp.einsum("bhd,bhde->bhe", queries, memory, precision=lax.Precision.HIGHEST)
    readout = scores[..., None] * values + keep_old[..., None] * read_old
    memory_next = (
        keep_old[..., None, None] * memory
        + write_new[..., None, None] * keys_scaled[..., :, None] * values[..., None, :]
    )
    return (readout, memory_next, new_max)


def head_mix(readout, head_gain, out_pre):
    scaled = readout * lax.rsqrt(jnp.mean(readout * readout, -1, keepdims=True) + 1e-06)
    flat_heads = scaled.reshape(scaled.shape[0], -1)
    return (flat_heads * head_gain * jax.nn.sigmoid(out_pre)).astype(jnp.bfloat16)


def route_weights(mid_float, w_group_router, w_expert_router, expert_route):
    group_logits = jnp.dot(
        mid_float, w_group_router.astype(jnp.float32), precision=lax.Precision.HIGHEST
    )
    expert_logits = jnp.dot(
        mid_float, w_expert_router.astype(jnp.float32), precision=lax.Precision.HIGHEST
    )
    first_expert = expert_route[:, 0]
    second_expert = expert_route[:, 1]
    expert_ids = lax.broadcasted_iota(jnp.int32, expert_logits.shape, 1)
    group_ids = lax.broadcasted_iota(jnp.int32, group_logits.shape, 1)
    first_logit = jnp.sum(jnp.where(expert_ids == first_expert[:, None], expert_logits, 0.0), -1)
    second_logit = jnp.sum(jnp.where(expert_ids == second_expert[:, None], expert_logits, 0.0), -1)
    group_pick = jnp.sum(
        jnp.where(group_ids == (first_expert // GROUP_SIZE)[:, None], group_logits, 0.0), -1
    )
    group_gate = jax.nn.sigmoid(group_pick)
    return (
        group_gate * jax.nn.sigmoid(first_logit - second_logit),
        group_gate * jax.nn.sigmoid(second_logit - first_logit),
    )


def slot_ranks(flat_routes, expert_total):
    onehot = (
        flat_routes[:, None]
        == lax.broadcasted_iota(jnp.int32, (flat_routes.shape[0], expert_total), 1)
    ).astype(jnp.int32)
    running = jnp.cumsum(onehot, 0)
    return jnp.sum((running - 1) * onehot, -1)


def body(
    hidden_in,
    w_query,
    w_key,
    w_value,
    w_outgate,
    w_igate,
    w_fgate,
    input_bias,
    forget_bias,
    mem_state,
    max_state,
    head_gain,
    w_output,
    first_gain,
    w_group_router,
    w_expert_router,
    expert_route,
    w_expgate,
    w_expup,
    w_expdown,
    second_gain,
):
    own_rows, width = hidden_in.shape
    heads_here = mem_state.shape[1]
    head_width = heads_here * DH
    top_count = expert_route.shape[1]
    spread_rows = lax.all_to_all(hidden_in, "ep", split_axis=1, concat_axis=0, tiled=True)
    stacked_w = jnp.concatenate([w_query, w_key, w_value, w_outgate], 1)
    gate_w = jnp.concatenate([w_igate, w_fgate], 1)
    proj_terms = jnp.dot(spread_rows, stacked_w, preferred_element_type=jnp.float32)
    gate_terms = jnp.dot(spread_rows, gate_w, preferred_element_type=jnp.float32)
    projected, gate_sums = (
        lax.psum_scatter(proj_terms, "ep", scatter_dimension=0, tiled=True),
        lax.psum_scatter(gate_terms, "ep", scatter_dimension=0, tiled=True),
    )
    shaped = projected.reshape(own_rows, 4, heads_here, DH)
    queries = shaped[:, 0]
    keys_raw = shaped[:, 1]
    values = shaped[:, 2]
    out_pre = shaped[:, 3].reshape(own_rows, head_width)
    input_sum = gate_sums[:, :heads_here]
    forget_sum = gate_sums[:, heads_here:]
    keys_scaled = keys_raw * DH ** (-0.5)
    log_input = input_sum + input_bias
    log_forget = jax.nn.log_sigmoid(forget_sum + forget_bias)
    memory = mem_state.reshape(own_rows, heads_here, DH, DH)
    readout, memory_square, new_max = mlstm_step(
        queries, keys_scaled, values, log_input, log_forget, memory, max_state
    )
    memory_next = memory_square.reshape(own_rows, heads_here, DH * DH)
    mixed_heads = head_mix(readout, head_gain, out_pre)
    partial_mix = jnp.dot(mixed_heads, w_output, preferred_element_type=jnp.float32).astype(
        jnp.bfloat16
    )
    mix = lax.psum(partial_mix.astype(jnp.float32).astype(jnp.bfloat16), "tp").astype(jnp.float32)
    mid_float = layer_norm(res_alpha * hidden_in.astype(jnp.float32) + mix, first_gain)
    mid = mid_float.astype(jnp.bfloat16)
    first_weight, second_weight = route_weights(
        mid_float, w_group_router, w_expert_router, expert_route
    )
    expert_total = w_expgate.shape[0] * lax.axis_size("ep")
    capacity = 2 * own_rows * top_count // expert_total
    flat_routes = expert_route.reshape(-1)
    local_slot = flat_routes * capacity + slot_ranks(flat_routes, expert_total)
    share_width = width // lax.axis_size("tp")
    mid_share = lax.dynamic_slice_in_dim(mid, lax.axis_index("tp") * share_width, share_width, 1)
    buffer = (
        jnp.zeros((expert_total * capacity, width), jnp.bfloat16)
        .at[local_slot]
        .set(jnp.repeat(mid, top_count, 0))
    )
    arrived = lax.all_to_all(
        buffer.reshape(expert_total, capacity, width), "ep", split_axis=0, concat_axis=1, tiled=True
    )
    gate_pre = jnp.einsum("erd,edf->erf", arrived, w_expgate, preferred_element_type=jnp.float32)
    up_pre = jnp.einsum("erd,edf->erf", arrived, w_expup, preferred_element_type=jnp.float32)
    hidden_units = (jax.nn.silu(gate_pre) * up_pre).astype(jnp.bfloat16)
    down_terms = jnp.einsum(
        "erf,efd->erd", hidden_units, w_expdown, preferred_element_type=jnp.float32
    ).astype(jnp.bfloat16)
    expert_share = lax.psum_scatter(
        down_terms.astype(jnp.float32).astype(jnp.bfloat16), "tp", scatter_dimension=2, tiled=True
    )
    returned = lax.all_to_all(expert_share, "ep", split_axis=1, concat_axis=0, tiled=True)
    picked = returned.reshape(expert_total * capacity, share_width)[local_slot]
    picked = picked.astype(jnp.float32).reshape(own_rows, top_count, share_width)
    moe = first_weight[:, None] * picked[:, 0] + second_weight[:, None] * picked[:, 1]
    joined = res_alpha * mid_share.astype(jnp.float32) + moe
    row_sum, square_sum = lax.psum((jnp.sum(joined, -1), jnp.sum(joined * joined, -1)), "tp")
    row_mean = row_sum / D
    row_var = square_sum / D - row_mean * row_mean
    hidden_out = (
        (joined - row_mean[:, None]) * lax.rsqrt(row_var[:, None] + 1e-05) * second_gain
    ).astype(jnp.bfloat16)
    return (hidden_out, memory_next, new_max)


def solution(mesh):
    return jax.shard_map(
        body,
        mesh=mesh,
        in_specs=(
            P("ep", None),
            P("ep", "tp"),
            P("ep", "tp"),
            P("ep", "tp"),
            P("ep", "tp"),
            P("ep", "tp"),
            P("ep", "tp"),
            P("tp"),
            P("tp"),
            P("ep", "tp", None),
            P("ep", "tp"),
            P("tp"),
            P("tp", None),
            P(),
            P(),
            P(),
            P("ep", None),
            P("ep", None, "tp"),
            P("ep", None, "tp"),
            P("ep", "tp", None),
            P("tp"),
        ),
        out_specs=(P("ep", "tp"), P("ep", "tp", None), P("ep", "tp")),
        check_vma=False,
    )
```

profile of v0, /device:TPU:0, one launch (start us, length us, event | category | flops | bytes accessed | tf_op | source)
XLA Modules:
  0.0 277.9 jit_solution(14590576950777728029)
XLA Ops:
  7.2 1.1 copy.139
  8.3 14.4 %all_to_all.37 = bf16[16,8,512]{2,0,1:T(8,128)(2,1)S(1)} all-to-all(bf16[16,8,512]{2,0,1:T(8,128)(2,1)S(1)} %bitcast.124), channel_id=1, replica_groups=mesh['ep'=8,'tp'=4] {'ep'}, dimensions={1} | all-to-all | bytes 262144 | tf_op jit(solution)/shard_map/all_to_all | solution.py:99
  22.7 0.8 convolution_bitcast_fusion.1
  23.5 0.7 copy.106
  24.4 2.3 convolution_bitcast_fusion
  26.6 1.3 copy.104
  28.1 6.1 %reshape.183 = f32[16,4,128,128]{3,2,1,0:T(8,128)} reshape(f32[16,4,16384]{2,1,0:T(4,128)} %param.30) | data formatting | bytes 8388608 | tf_op jit(solution)/shard_map/reshape | solution.py:118
  34.7 0.2 select_reduce_fusion
  34.9 49.9 %reduce-scatter.12.cloned.1.call-done = f32[16,8]{1,0:T(8,128)} async-done(((f32[128,8]{1,0:T(8,128)}), f32[16,8]{1,0:T(8,128)}) %reduce-scatter.12.cloned.1.call-update) | async-done | bytes 528 | tf_op jit(solution)/shard_map/reduce_scatter | solution.py:106
  84.8 0.9 broadcast_multiply_fusion.2
  85.7 66.2 %reduce-scatter.10.cloned.1.call-done = f32[16,2048]{1,0:T(8,128)} async-done(((f32[128,2048]{1,0:T(8,128)}), f32[16,2048]{1,0:T(8,128)}) %reduce-scatter.10.cloned.1.call-update) | async-done | bytes 131088
  151.8 1.2 copy.105
  153.1 0.9 fusion.62
  154.0 1.0 copy.109
  155.1 1.1 copy.110
  156.1 1.1 copy.111
  157.2 0.1 bitcast_multiply_fusion.2
  157.3 5.3 %fusion.64 = f32[16,4,1,128]{3,2,1,0:T(1,128)S(1)} fusion(f32[16,4,128,1]{2,3,1,0:T(1,128)S(1)} %bitcast.125, f32[16,4,128,128]{3,2,1,0:T(8,128)} %reshape.183), kind=kOutput, calls=%fused_computation.111 | convolution fusion | flops 12582912 | bytes 4259840 | tf_op jit(solution)/shard_map/bhd,bhde->bhe/dot_general | solution.py:25
  162.8 0.2 multiply_reduce_fusion.2
  163.0 0.1 broadcast_multiply_fusion.1
  163.3 3.5 %convolution_convert_fusion.1 = bf16[16,4096]{1,0:T(8,128)(2,1)} fusion(bf16[512,4096]{1,0:T(8,128)(2,1)} %param.33, f32[2,8,4,128]{3,2,1,0:T(4,128)S(1)} %bitcast.128, f32[2,8,4,128]{3,2,1,0:T(4,128)S(1)} %bitcast.129, f32[512]{0:T(512)S(1)} %copy-done.7), kind=kOutput, calls=%fused_computation.4 | convolution fusion | flops 67198976 | bytes 4392960 | tf_op jit(solution)/shard_map/dot_general | solution.py:124
  166.8 30.9 %all-reduce.3.cloned.1.call-done = bf16[16,4096]{1,0:T(8,128)(2,1)} async-done(((bf16[16,4096]{1,0:T(8,128)(2,1)}), bf16[16,4096]{1,0:T(8,128)(2,1)}) %all-reduce.3.cloned.1.call-update) | async-done | bytes 131088 | tf_op jit(solution)/shard_map/psum | solution.py:127
  197.7 1.1 fusion.27
  198.8 1.0 fusion.58
  199.8 0.2 broadcast_in_dim.15
  200.1 1.8 scatter_custom_fusion
  201.9 5.5 %all-to-all-start.1 = ((bf16[8,8,4096]{2,1,0:T(8,128)(2,1)}), bf16[8,8,4096]{2,1,0:T(8,128)(2,1)S(1)}, u32[]{:S(2)}, u32[]{:S(2)}) async-start(bf16[8,8,4096]{2,1,0:T(8,128)(2,1)} %bitcast.18), calls=%async_computation.1 | async-start | bytes 1048576 | tf_op jit(solution)/shard_map/all_to_all | solution.py:144
  207.5 0.7 copy.98
  208.1 2.6 broadcast_multiply_fusion
  210.8 5.6 %mul.268 = f32[16,4,16384]{2,1,0:T(4,128)} reshape(f32[16,4,128,128]{3,2,1,0:T(8,128)} %broadcast_multiply_fusion) | data formatting | bytes 8388608 | tf_op jit(solution)/shard_map/mul | solution.py:29
  216.3 4.5 %all-to-all-done.1 = bf16[8,8,4096]{2,1,0:T(8,128)(2,1)S(1)} async-done(((bf16[8,8,4096]{2,1,0:T(8,128)(2,1)}), bf16[8,8,4096]{2,1,0:T(8,128)(2,1)S(1)}, u32[]{:S(2)}, u32[]{:S(2)}) %all-to-all-start.1) | async-done | bytes 524320 | tf_op jit(solution)/shard_map/all_to_all | solution.py:144
  220.8 2.0 fusion.11
  222.9 3.8 %fusion = bf16[1,64,4096]{2,1,0:T(8,128)(2,1)} fusion(bf16[1,256,4096]{2,1,0:T(8,128)(2,1)S(1)} %copy-done, bf16[1,4096,256]{2,1,0:T(8,128)(2,1)} %param.39, bf16[8,8,4096]{2,1,0:T(8,128)(2,1)S(1)} %all-to-all-done.1, f32[64,256]{1,0:T(8,128)S(1)} %fusion.11), kind=kOutput, calls=%fused_computation.3 | convolution fusion | flops 268795904 | bytes 5308416 | tf_op jit(solution)/shard_map/erf,efd->erd/dot_general | solution.py:150
  226.7 6.9 %multiply_add_fusion = f32[16,4,16384]{2,1,0:T(4,128)} fusion(f32[16,4,16384]{2,1,0:T(4,128)} %mul.268, f32[16,4,16384]{2,1,0:T(4,128)} %param.30, f32[16,4]{1,0:T(8,128)S(1)} %get-tuple-element.28), kind=kLoop, calls=%fused_computation.5 | loop fusion | flops 2097152 | bytes 12583168 | tf_op jit(solution)/shard_map/add | solution.py:28
  233.6 0.4 fusion.19
  234.0 0.4 select_reduce_fusion.2
  234.4 12.5 %reduce-scatter.8.cloned.1.call-done = bf16[1,64,1024]{2,1,0:T(8,128)(2,1)} async-done(((bf16[1,64,4096]{2,1,0:T(8,128)(2,1)}), bf16[1,64,1024]{2,1,0:T(8,128)(2,1)}) %reduce-scatter.8.cloned.1.call-update) | async-done | bytes 131088 | tf_op jit(solution)/shard_map/reduce_scatter | solution.py:153
  246.9 1.1 copy.141
  248.0 0.5 broadcast.198
  248.5 1.4 reduce
  249.9 0.7 reshape.217
  250.6 5.5 %all-to-all-start.2 = ((bf16[8,2,4096]{2,1,0:T(2,128)(2,1)}), bf16[8,2,4096]{2,1,0:T(2,128)(2,1)S(1)}, u32[]{:S(2)}, u32[]{:S(2)}) async-start(bf16[8,2,4096]{2,1,0:T(2,128)(2,1)} %reshape.217), calls=%async_computation.3 | async-start | bytes 262144 | tf_op jit(solution)/shard_map/all_to_all | solution.py:156
  256.2 7.3 %all-to-all-done.2 = bf16[8,2,4096]{2,1,0:T(2,128)(2,1)S(1)} async-done(((bf16[8,2,4096]{2,1,0:T(2,128)(2,1)}), bf16[8,2,4096]{2,1,0:T(2,128)(2,1)S(1)}, u32[]{:S(2)}, u32[]{:S(2)}) %all-to-all-start.2) | async-done | bytes 131104 | tf_op jit(solution)/shard_map/all_to_all | solution.py:156
  263.5 0.1 reshape.218
  263.7 0.6 gather_fusion
  264.5 0.2 fusion.59
  264.7 5.9 %all-reduce = (f32[16]{0:T(128)S(1)}, f32[16]{0:T(128)S(1)}) all-reduce(f32[16]{0:T(128)S(1)} %get-tuple-element.9, f32[16]{0:T(128)S(1)} %get-tuple-element.8), channel_id=1, replica_groups=mesh['ep'=8,'tp'=4] {'tp'}, use_global_device_ids=true, to_apply=%region_17.18 | all-reduce | flops 32 | bytes 256 | tf_op jit(solution)/shard_map/psum | solution.py:161
  270.7 0.7 multiply_convert_fusion
  (58 shorter events, 1.5 us)
Async XLA Ops:
  7.2 215.7 %copy-start = (bf16[1,256,4096]{2,1,0:T(8,128)(2,1)S(1)}, bf16[1,256,4096]{2,1,0:T(8,128)(2,1)}, u32[]{:S(2)}) copy-start(bf16[1,256,4096]{2,1,0:T(8,128)(2,1)} %param.40) | copy-start | bytes 6291460
  7.2 77.6 %reduce-scatter.12.cloned.1.call-start = ((), (), s32[]{:S(2)}) async-start(), calls=%async_computation.9 | async-start | bytes 73728 | tf_op jit(solution)/shard_map/reduce_scatter | solution.py:106
  24.3 3.7 %copy-start.10 = (f32[16,4]{0,1:T(4,128)S(1)}, f32[16,4]{0,1:T(4,128)}, u32[]{:S(2)}) copy-start(f32[16,4]{0,1:T(4,128)} %param.31) | copy-start | bytes 772
  24.3 127.5 %reduce-scatter.10.cloned.1.call-start = ((), (), s32[]{:S(2)}) async-start(), calls=%async_computation.8 | async-start | bytes 1179648
  28.0 169.7 %all-reduce.3.cloned.1.call-start = ((), (), s32[]{:S(2)}) async-start(), calls=%async_computation.6 | async-start | bytes 262144 | tf_op jit(solution)/shard_map/psum | solution.py:127
  28.1 6.1 %copy-start.5 = (s32[16,2]{0,1:T(2,128)S(1)}, s32[16,2]{0,1:T(2,128)}, u32[]{:S(2)}) copy-start(s32[16,2]{0,1:T(2,128)} %param.37) | copy-start | bytes 388
  28.1 56.7 %copy-start.8 = (f32[4]{0:T(128)S(1)}, f32[4]{0:T(128)}, u32[]{:S(2)}) copy-start(f32[4]{0:T(128)} %param.28) | copy-start | bytes 52
  28.1 56.7 %copy-start.9 = (f32[4]{0:T(128)S(1)}, f32[4]{0:T(128)}, u32[]{:S(2)}) copy-start(f32[4]{0:T(128)} %param.29) | copy-start | bytes 52
  85.7 77.0 %copy-start.3 = (f32[16,8]{1,0:T(8,128)S(1)}, f32[16,8]{1,0:T(8,128)}, u32[]{:S(2)}) copy-start(f32[16,8]{1,0:T(8,128)} %reduce-scatter.12.cloned.1.call-done) | copy-start | bytes 1540
  153.1 10.2 %copy-start.7 = (f32[512]{0:T(512)S(1)}, f32[512]{0:T(512)}, u32[]{:S(2)}) copy-start(f32[512]{0:T(512)} %param.32) | copy-start | bytes 6148
  157.3 40.4 %copy-start.1 = (bf16[16,4096]{1,0:T(8,128)(2,1)S(1)}, bf16[16,4096]{1,0:T(8,128)(2,1)}, u32[]{:S(2)}) copy-start(bf16[16,4096]{1,0:T(8,128)(2,1)} %param.21) | copy-start | bytes 393220
  157.3 41.5 %copy-start.4 = (f32[4096]{0:T(1024)S(1)}, f32[4096]{0:T(1024)}, u32[]{:S(2)}) copy-start(f32[4096]{0:T(1024)} %param.34) | copy-start | bytes 49156
  201.9 18.9 %all-to-all-start.1 = ((bf16[8,8,4096]{2,1,0:T(8,128)(2,1)}), bf16[8,8,4096]{2,1,0:T(8,128)(2,1)S(1)}, u32[]{:S(2)}, u32[]{:S(2)}) async-start(bf16[8,8,4096]{2,1,0:T(8,128)(2,1)} %bitcast.18), calls=%async_computation.1 | async-start | bytes 1048576 | tf_op jit(solution)/shard_map/all_to_all | solution.py:144
  207.4 39.5 %reduce-scatter.8.cloned.1.call-start = ((), (), s32[]{:S(2)}) async-start(), calls=%async_computation.7 | async-start | bytes 655360 | tf_op jit(solution)/shard_map/reduce_scatter | solution.py:153
  226.7 6.9 %copy-start.2 = (bf16[16,4096]{1,0:T(8,128)(2,1)S(1)}, bf16[16,4096]{1,0:T(8,128)(2,1)}, u32[]{:S(2)}) copy-start(bf16[16,4096]{1,0:T(8,128)(2,1)} %all-reduce.3.cloned.1.call-done) | copy-start | bytes 393220
  226.7 6.9 %copy-start.12 = (bf16[4096,2]{0,1:T(2,128)(2,1)S(1)}, bf16[4096,2]{0,1:T(2,128)(2,1)}, u32[]{:S(2)}) copy-start(bf16[4096,2]{0,1:T(2,128)(2,1)} %param.35) | copy-start | bytes 49156
  226.7 7.3 %copy-start.11 = (bf16[4096,8]{0,1:T(8,128)(2,1)S(1)}, bf16[4096,8]{0,1:T(8,128)(2,1)}, u32[]{:S(2)}) copy-start(bf16[4096,8]{0,1:T(8,128)(2,1)} %param.36) | copy-start | bytes 196612
  233.6 37.1 %copy-start.6 = (f32[1024]{0:T(1024)S(1)}, f32[1024]{0:T(1024)}, u32[]{:S(2)}) copy-start(f32[1024]{0:T(1024)} %param.41) | copy-start | bytes 12292
  250.6 12.9 %all-to-all-start.2 = ((bf16[8,2,4096]{2,1,0:T(2,128)(2,1)}), bf16[8,2,4096]{2,1,0:T(2,128)(2,1)S(1)}, u32[]{:S(2)}, u32[]{:S(2)}) async-start(bf16[8,2,4096]{2,1,0:T(2,128)(2,1)} %reshape.217), calls=%async_computation.3 | async-start | bytes 262144 | tf_op jit(solution)/shard_map/all_to_all | solution.py:156
Sparse Core Ops, SparseCore 0:
  24.4 60.3 reduce-scatter.11
  88.2 63.5 reduce-scatter.9
  166.9 30.7 all-reduce.2
  226.8 20.0 reduce-scatter.7
where the time goes:
time: 279 us; the launch traced here: 278 us
  waiting for transfers between devices  171 us (61%)
  local copies, waits for them, and re-layouts  26.8 us (10%)
  blocking collectives  20.3 us (7%)
  matrix products  18.5 us (7%)
  other arithmetic  15.7 us (6%)
  between operations  14.1 us (5%)
  starting transfers between devices  11.2 us (4%)
    unnamed x5, waiting for transfers between devices  66.2 us
    reduce_scatter x1, waiting for transfers between devices, body(): lax.psum_scatter(gate_terms, 'ep', scatter_dimension=0, tiled=True)  49.9 us
    psum x1, waiting for transfers between devices, body(): lax.psum(partial_mix.astype(jnp.float32).astype(jnp.bfloat16), 'tp')  30.9 us
    all_to_all x1, blocking collectives, body(): lax.all_to_all(hidden_in, 'ep', split_axis=1, concat_axis=0, tiled=True)  14.4 us
    reduce_scatter x1, waiting for transfers between devices, body(): lax.psum_scatter(down_terms.astype(jnp.float32).astype(jnp.bfloat16), 'tp...  12.5 us
    unnamed x40, local copies, waits for them, and re-layouts  8.86 us
    all_to_all x1, waiting for transfers between devices, body(): lax.all_to_all(expert_share, 'ep', split_axis=1, concat_axis=0, tiled=True)  7.32 us
    add x1, other arithmetic, mlstm_step(): keep_old[..., None, None] * memory  6.88 us
  transfers between devices with their start and end apart: 6, of which 6 were waited for; matrix products, arithmetic and copies ran while one was open for 10% of the time, Pallas kernels for 0%

commit v1 on v0

--- a/solution.py
+++ b/solution.py
@@ -1,11 +1,16 @@
+import functools
+
 import jax
 import jax.numpy as jnp
 from jax import lax
+from jax.experimental import pallas as pl
+from jax.experimental.pallas import tpu as pltpu
 from jax.sharding import PartitionSpec as P
 
 D = 4096
 DH = 128
 GROUP_SIZE = 4
+MESH = pl.DeviceIdType.MESH
 
 
 res_alpha = 8.0**0.25
@@ -167,9 +172,489 @@
     return (hidden_out, memory_next, new_max)
 
 
+def greet(peers):
+    barrier = pltpu.get_barrier_semaphore()
+    for peer in peers:
+        pl.semaphore_signal(barrier, inc=1, device_id=peer, device_id_type=MESH)
+    pl.semaphore_wait(barrier, len(peers))
+
+
+def remote(source, target, send_sem, recv_sem, peer):
+    return pltpu.make_async_remote_copy(
+        src_ref=source,
+        dst_ref=target,
+        send_sem=send_sem,
+        recv_sem=recv_sem,
+        device_id=peer,
+        device_id_type=MESH,
+    )
+
+
+def project_kernel(
+    n_ep,
+    hidden,
+    gate_w,
+    wq,
+    wk,
+    wv,
+    wo,
+    proj_out,
+    gate_out,
+    weights,
+    spread,
+    half_send,
+    half_recv,
+    full_send,
+    full_recv,
+    gate_send,
+    gate_recv,
+    load_sem,
+    h_send,
+    h_recv,
+    v_send,
+    v_recv,
+    q_send,
+    q_recv,
+    g_send,
+    g_recv,
+):
+    me = lax.axis_index("ep")
+    tp = lax.axis_index("tp")
+    rows = hidden.shape[0]
+    depth, cols = wq.shape
+    loads = [pltpu.make_async_copy(w, weights.at[i], load_sem.at[i]) for i, w in enumerate((wq, wk, wv, wo))]
+    for load in loads:
+        load.start()
+    after = [(lax.rem(me + o, n_ep), tp) for o in range(n_ep)]
+    before = [(lax.rem(me + n_ep - o, n_ep), tp) for o in range(n_ep)]
+    greet(after[1:])
+    sent = []
+    for o in range(1, n_ep):
+        columns = pl.ds(pl.multiple_of(after[o][0] * depth, depth), depth)
+        copy = remote(hidden.at[:, columns], spread.at[o], h_send.at[o], h_recv.at[o], after[o])
+        copy.start()
+        sent.append(copy)
+    spread[0] = hidden[:, pl.ds(pl.multiple_of(me * depth, depth), depth)]
+    for load in loads:
+        load.wait()
+    for copy in sent:
+        copy.wait_recv()
+    lhs = spread[...].reshape(n_ep * rows, depth)
+    gates = jnp.dot(lhs, gate_w[...], preferred_element_type=jnp.float32)
+    gate_send[...] = gates.reshape(n_ep, rows, gates.shape[1])
+    gate_copies = [remote(gate_send.at[o], gate_recv.at[o], g_send.at[o], g_recv.at[o], before[o]) for o in range(1, n_ep)]
+    for copy in gate_copies:
+        copy.start()
+    for i in range(2):
+        part = jnp.dot(lhs, weights[2 + i], preferred_element_type=jnp.float32)
+        half_send[:, :, i * cols : (i + 1) * cols] = part.astype(jnp.bfloat16).reshape(n_ep, rows, cols)
+    half_copies = [remote(half_send.at[o], half_recv.at[o], v_send.at[o], v_recv.at[o], before[o]) for o in range(1, n_ep)]
+    for copy in half_copies:
+        copy.start()
+    for i in range(2):
+        part = jnp.dot(lhs, weights[i], preferred_element_type=jnp.float32)
+        full_send[:, :, i * cols : (i + 1) * cols] = part.reshape(n_ep, rows, cols)
+    full_copies = [remote(full_send.at[o], full_recv.at[o], q_send.at[o], q_recv.at[o], before[o]) for o in range(1, n_ep)]
+    for copy in full_copies:
+        copy.start()
+    gate_total = gate_send[0]
+    half_part = slice(2 * cols, 4 * cols)
+    full_part = slice(0, 2 * cols)
+    proj_out[:, half_part] = half_send[0].astype(jnp.float32)
+    proj_out[:, full_part] = full_send[0]
+    for o in range(1, n_ep):
+        gate_copies[o - 1].wait_recv()
+        gate_total += gate_recv[o]
+        half_copies[o - 1].wait_recv()
+        proj_out[:, half_part] += half_recv[o].astype(jnp.float32)
+    for o in range(1, n_ep):
+        full_copies[o - 1].wait_recv()
+        proj_out[:, full_part] += full_recv[o]
+    gate_out[...] = gate_total
+    for copy in sent + gate_copies + half_copies + full_copies:
+        copy.wait_send()
+
+
+def project(n_ep, hidden, gate_w, wq, wk, wv, wo):
+    rows = hidden.shape[0]
+    depth, cols = wq.shape
+    vmem = pl.BlockSpec(memory_space=pltpu.VMEM)
+    anywhere = pl.BlockSpec(memory_space=pl.ANY)
+    sems = pltpu.SemaphoreType.DMA((n_ep,))
+    return pl.pallas_call(
+        functools.partial(project_kernel, n_ep),
+        out_shape=(
+            jax.ShapeDtypeStruct((rows, 4 * cols), jnp.float32),
+            jax.ShapeDtypeStruct((rows, gate_w.shape[1]), jnp.float32),
+        ),
+        in_specs=[vmem, vmem] + [anywhere] * 4,
+        out_specs=(vmem, vmem),
+        scratch_shapes=[
+            pltpu.VMEM((4, depth, cols), jnp.bfloat16),
+            pltpu.VMEM((n_ep, rows, depth), jnp.bfloat16),
+            pltpu.VMEM((n_ep, rows, 2 * cols), jnp.bfloat16),
+            pltpu.VMEM((n_ep, rows, 2 * cols), jnp.bfloat16),
+            pltpu.VMEM((n_ep, rows, 2 * cols), jnp.float32),
+            pltpu.VMEM((n_ep, rows, 2 * cols), jnp.float32),
+            pltpu.VMEM((n_ep, rows, gate_w.shape[1]), jnp.float32),
+            pltpu.VMEM((n_ep, rows, gate_w.shape[1]), jnp.float32),
+            pltpu.SemaphoreType.DMA((4,)),
+        ]
+        + [sems] * 8,
+        compiler_params=pltpu.CompilerParams(collective_id=0, has_side_effects=True),
+        name="project",
+    )(hidden, gate_w, wq, wk, wv, wo)
+
+
+def cell_kernel(proj, keep_ref, write_ref, gain_ref, mem_ref, mixed_ref, mem_out):
+    heads = mem_ref.shape[1]
+    queries = proj[0, 0:heads]
+    keys = proj[0, heads : 2 * heads] * DH ** (-0.5)
+    values = proj[0, 2 * heads : 3 * heads]
+    out_pre = proj[0, 3 * heads : 4 * heads]
+    keep = keep_ref[0]
+    write = write_ref[0]
+    write_keys = keys * write
+    read_old = jnp.zeros_like(queries)
+    for d in range(DH):
+        block = mem_ref[0, :, d * DH : (d + 1) * DH]
+        read_old += queries[:, d : d + 1] * block
+        mem_out[0, :, d * DH : (d + 1) * DH] = keep * block + write_keys[:, d : d + 1] * values
+    scores = jnp.sum(queries * keys, -1, keepdims=True) * write
+    readout = scores * values + keep * read_old
+    scaled = readout * lax.rsqrt(jnp.mean(readout * readout, -1, keepdims=True) + 1e-06)
+    mixed_ref[0] = (scaled * gain_ref[...] * jax.nn.sigmoid(out_pre)).astype(jnp.bfloat16)
+
+
+def cell(proj, keep, write, gain, memory):
+    rows, heads, flat = memory.shape
+    one = lambda *dims: pl.BlockSpec((1,) + dims, lambda b: (b,) + (0,) * len(dims))
+    return pl.pallas_call(
+        cell_kernel,
+        grid=(rows,),
+        out_shape=(
+            jax.ShapeDtypeStruct((rows, heads, DH), jnp.bfloat16),
+            jax.ShapeDtypeStruct((rows, heads, flat), jnp.float32),
+        ),
+        in_specs=[
+            one(4 * heads, DH),
+            one(heads, DH),
+            one(heads, DH),
+            pl.BlockSpec((heads, DH), lambda b: (0, 0)),
+            one(heads, flat),
+        ],
+        out_specs=(one(heads, DH), one(heads, flat)),
+        name="cell",
+    )(proj, keep, write, gain, memory)
+
+
+def moe_kernel(
+    n_ep,
+    n_tp,
+    groups,
+    mixed,
+    hidden,
+    gain1,
+    gain2,
+    router_t,
+    route,
+    perm,
+    perm_t,
+    w_out,
+    w_gate,
+    w_up,
+    w_down,
+    out_ref,
+    wo_buf,
+    wg_buf,
+    wu_buf,
+    wd_buf,
+    mix_send,
+    mix_recv,
+    mid_buf,
+    arrived,
+    down_send,
+    down_recv,
+    ret_send,
+    ret_recv,
+    stat_send,
+    stat_recv,
+    load_sem,
+    m_send,
+    m_recv,
+    a_send,
+    a_recv,
+    d_send,
+    d_recv,
+    r_send,
+    r_recv,
+    s_send,
+    s_recv,
+):
+    me = lax.axis_index("ep")
+    tp = lax.axis_index("tp")
+    rows, width = hidden.shape
+    share = width // n_tp
+    block = rows // groups
+    loads = [
+        pltpu.make_async_copy(w_out, wo_buf, load_sem.at[0]),
+        pltpu.make_async_copy(w_gate.at[0], wg_buf, load_sem.at[1]),
+        pltpu.make_async_copy(w_up.at[0], wu_buf, load_sem.at[2]),
+        pltpu.make_async_copy(w_down.at[0], wd_buf, load_sem.at[3]),
+    ]
+    for load in loads:
+        load.start()
+    ep_after = [(lax.rem(me + o, n_ep), tp) for o in range(n_ep)]
+    ep_before = [(lax.rem(me + n_ep - o, n_ep), tp) for o in range(n_ep)]
+    tp_after = [(me, lax.rem(tp + o, n_tp)) for o in range(n_tp)]
+    greet(ep_after[1:] + tp_after[1:])
+    started = []
+
+    def begin(copies):
+        for copy in copies:
+            copy.start()
+        started.extend(copies)
+        return copies
+
+    mixed_sorted = jnp.dot(perm[...], mixed[...], preferred_element_type=jnp.float32).astype(jnp.bfloat16)
+    loads[0].wait()
+    for c in range(n_tp):
+        columns = slice(c * share, (c + 1) * share)
+        mix_send[:, columns] = jnp.dot(
+            mixed_sorted, wo_buf[:, columns], preferred_element_type=jnp.float32
+        ).astype(jnp.bfloat16)
+    copies = begin(
+        [remote(mix_send, mix_recv.at[o], m_send.at[o], m_recv.at[o], tp_after[o]) for o in range(1, n_tp)]
+    )
+    joined = res_alpha * jnp.dot(perm[...], hidden[...], preferred_element_type=jnp.float32)
+    joined += mix_send[...].astype(jnp.float32)
+    for o in range(1, n_tp):
+        copies[o - 1].wait_recv()
+        joined += mix_recv[o].astype(jnp.float32)
+    mid_float = layer_norm(joined, gain1[...])
+    for g in range(groups):
+        mid_buf[g] = mid_float[g * block : (g + 1) * block].astype(jnp.bfloat16)
+    copies = begin(
+        [
+            remote(
+                mid_buf.at[lax.div(ep_after[o][0], GROUP_SIZE)],
+                arrived.at[o],
+                a_send.at[o],
+                a_recv.at[o],
+                ep_after[o],
+            )
+            for o in range(1, n_ep)
+        ]
+    )
+    high = mid_float.astype(jnp.bfloat16)
+    rest = mid_float - high.astype(jnp.float32)
+    middle = rest.astype(jnp.bfloat16)
+    low = (rest - middle.astype(jnp.float32)).astype(jnp.bfloat16)
+    logits = jnp.zeros((rows, router_t.shape[0]), jnp.float32)
+    for piece in (low, middle, high):
+        logits += lax.dot_general(
+            piece, router_t[...], (((1,), (1,)), ((), ())), preferred_element_type=jnp.float32
+        )
+    first = route[:, 0:1]
+    second = route[:, 1:2]
+    lanes = lax.broadcasted_iota(jnp.int32, logits.shape, 1)
+    pick = lambda index: jnp.sum(jnp.where(lanes == index, logits, 0.0), -1, keepdims=True)
+    first_logit = pick(first)
+    second_logit = pick(second)
+    group_gate = jax.nn.sigmoid(pick(n_ep + lax.shift_right_logical(first, 2)))
+    weight1 = group_gate * jax.nn.sigmoid(first_logit - second_logit)
+    weight2 = group_gate * jax.nn.sigmoid(second_logit - first_logit)
+    arrived[0] = mid_buf[lax.div(me, GROUP_SIZE)]
+    loads[1].wait()
+    loads[2].wait()
+    for copy in copies:
+        copy.wait_recv()
+    tokens = arrived[...].astype(jnp.float32).reshape(n_ep * block, width).astype(jnp.bfloat16)
+    gate_pre = jnp.dot(tokens, wg_buf[...], preferred_element_type=jnp.float32)
+    up_pre = jnp.dot(tokens, wu_buf[...], preferred_element_type=jnp.float32)
+    units = (gate_pre * jax.nn.sigmoid(gate_pre) * up_pre).astype(jnp.bfloat16)
+    loads[3].wait()
+    copies = []
+    for o in list(range(1, n_tp)) + [0]:
+        columns = pl.ds(pl.multiple_of(tp_after[o][1] * share, share), share)
+        down_send[o] = jnp.dot(units, wd_buf[:, columns], preferred_element_type=jnp.float32).astype(
+            jnp.bfloat16
+        )
+        if o:
+            copies += begin(
+                [remote(down_send.at[o], down_recv.at[o], d_send.at[o], d_recv.at[o], tp_after[o])]
+            )
+    total = down_send[0].astype(jnp.float32)
+    for o in range(1, n_tp):
+        copies[o - 1].wait_recv()
+        total += down_recv[o].astype(jnp.float32)
+    for o in range(n_ep):
+        ret_send[o] = total[o * block : (o + 1) * block].astype(jnp.bfloat16)
+    copies = begin(
+        [
+            remote(ret_send.at[o], ret_recv.at[o], r_send.at[o], r_recv.at[o], ep_before[o])
+            for o in range(1, n_ep)
+        ]
+    )
+    mine = pl.ds(pl.multiple_of(tp * share, share), share)
+    joined = res_alpha * mid_buf[:, :, mine].astype(jnp.float32).reshape(rows, share)
+    for o in range(n_ep):
+        expert = ep_after[o][0]
+        if o:
+            copies[o - 1].wait_recv()
+        result = (ret_recv[o] if o else ret_send[0]).astype(jnp.float32)
+        weight = jnp.where(first == expert, weight1, 0.0) + jnp.where(second == expert, weight2, 0.0)
+        joined += weight * jnp.concatenate([result] * groups, 0)
+    row_sum = jnp.sum(joined, -1, keepdims=True)
+    square_sum = jnp.sum(joined * joined, -1, keepdims=True)
+    stat_send[0] = jnp.broadcast_to(row_sum, stat_send.shape[1:])
+    stat_send[1] = jnp.broadcast_to(square_sum, stat_send.shape[1:])
+    copies = begin(
+        [remote(stat_send, stat_recv.at[o], s_send.at[o], s_recv.at[o], tp_after[o]) for o in range(1, n_tp)]
+    )
+    for o in range(1, n_tp):
+        copies[o - 1].wait_recv()
+        row_sum += stat_recv[o, 0][:, 0:1]
+        square_sum += stat_recv[o, 1][:, 0:1]
+    row_mean = row_sum / width
+    row_var = square_sum / width - row_mean * row_mean
+    result = ((joined - row_mean) * lax.rsqrt(row_var + 1e-05) * gain2[...]).astype(jnp.bfloat16)
+    out_ref[...] = jnp.dot(perm_t[...], result, preferred_element_type=jnp.float32).astype(jnp.bfloat16)
+    for copy in started:
+        copy.wait_send()
+
+
+def mix_and_moe(n_ep, n_tp, groups, *operands):
+    mixed, hidden = operands[:2]
+    w_out, w_gate, w_up, w_down = operands[-4:]
+    rows, width = hidden.shape
+    share = width // n_tp
+    block = rows // groups
+    vmem = pl.BlockSpec(memory_space=pltpu.VMEM)
+    anywhere = pl.BlockSpec(memory_space=pl.ANY)
+    ep_sems = pltpu.SemaphoreType.DMA((n_ep,))
+    tp_sems = pltpu.SemaphoreType.DMA((n_tp,))
+    half = jnp.bfloat16
+    return pl.pallas_call(
+        functools.partial(moe_kernel, n_ep, n_tp, groups),
+        out_shape=jax.ShapeDtypeStruct((rows, share), half),
+        in_specs=[vmem] * (len(operands) - 4) + [anywhere] * 4,
+        out_specs=vmem,
+        scratch_shapes=[
+            pltpu.VMEM(w_out.shape, half),
+            pltpu.VMEM(w_gate.shape[1:], half),
+            pltpu.VMEM(w_up.shape[1:], half),
+            pltpu.VMEM(w_down.shape[1:], half),
+            pltpu.VMEM((rows, width), half),
+            pltpu.VMEM((n_tp, rows, width), half),
+            pltpu.VMEM((groups, block, width), half),
+            pltpu.VMEM((n_ep, block, width), half),
+            pltpu.VMEM((n_tp, n_ep * block, share), half),
+            pltpu.VMEM((n_tp, n_ep * block, share), half),
+            pltpu.VMEM((n_ep, block, share), half),
+            pltpu.VMEM((n_ep, block, share), half),
+            pltpu.VMEM((2, rows, DH), jnp.float32),
+            pltpu.VMEM((n_tp, 2, rows, DH), jnp.float32),
+            pltpu.SemaphoreType.DMA((4,)),
+            tp_sems,
+            tp_sems,
+            ep_sems,
+            ep_sems,
+            tp_sems,
+            tp_sems,
+            ep_sems,
+            ep_sems,
+            tp_sems,
+            tp_sems,
+        ],
+        compiler_params=pltpu.CompilerParams(collective_id=1, has_side_effects=True),
+        name="mix_and_moe",
+    )(*operands)
+
+
+def kernel_body(
+    hidden_in,
+    w_query,
+    w_key,
+    w_value,
+    w_outgate,
+    w_igate,
+    w_fgate,
+    input_bias,
+    forget_bias,
+    mem_state,
+    max_state,
+    head_gain,
+    w_output,
+    first_gain,
+    w_group_router,
+    w_expert_router,
+    expert_route,
+    w_expgate,
+    w_expup,
+    w_expdown,
+    second_gain,
+):
+    n_ep, n_tp = lax.axis_size("ep"), lax.axis_size("tp")
+    rows, width = hidden_in.shape
+    heads = mem_state.shape[1]
+    groups = w_group_router.shape[1]
+    gate_w = jnp.concatenate([w_igate, w_fgate], 1)
+    gate_w = jnp.pad(gate_w, ((0, 0), (0, DH - 2 * heads)))
+    projected, gate_sums = project(n_ep, hidden_in, gate_w, w_query, w_key, w_value, w_outgate)
+    log_input = gate_sums[:, :heads] + input_bias
+    log_forget = jax.nn.log_sigmoid(gate_sums[:, heads : 2 * heads] + forget_bias)
+    new_max = jnp.maximum(log_forget + max_state, log_input)
+    keep_old = jnp.exp(log_forget + max_state - new_max)
+    write_new = jnp.exp(log_input - new_max)
+    spread_gate = lambda gate: jnp.broadcast_to(gate[:, :, None], (rows, heads, DH))
+    mixed, memory_next = cell(
+        projected.reshape(rows, 4 * heads, DH),
+        spread_gate(keep_old),
+        spread_gate(write_new),
+        head_gain.reshape(heads, DH),
+        mem_state,
+    )
+    row_ids = jnp.arange(rows, dtype=jnp.int32)
+    group = expert_route[:, 0] // GROUP_SIZE
+    earlier = (group[:, None] == group[None, :]) & (row_ids[None, :] < row_ids[:, None])
+    place = group * (rows // groups) + jnp.sum(earlier.astype(jnp.int32), 1)
+    perm = place[None, :] == row_ids[:, None]
+    route = jnp.sum(jnp.where(perm[:, :, None], expert_route[None], 0), 1)
+    router = jnp.concatenate([w_expert_router, w_group_router], 1)
+    router_t = jnp.pad(router, ((0, 0), (0, -router.shape[1] % 16))).T
+    hidden_out = mix_and_moe(
+        n_ep,
+        n_tp,
+        groups,
+        mixed.reshape(rows, heads * DH),
+        hidden_in,
+        first_gain[None],
+        second_gain[None],
+        router_t,
+        route,
+        perm.astype(jnp.bfloat16),
+        perm.T.astype(jnp.bfloat16),
+        w_output,
+        w_expgate,
+        w_expup,
+        w_expdown,
+    )
+    return (hidden_out, memory_next, new_max)
+
+
+def either_body(*operands):
+    hidden_in, w_query, group_router, experts = operands[0], operands[1], operands[14], operands[17]
+    rows, width = hidden_in.shape
+    block, odd_rows = divmod(rows, group_router.shape[1])
+    aligned = rows % 16 == 0 and block % 8 == 0 and odd_rows == 0 and experts.shape[0] == 1
+    aligned = aligned and w_query.shape[0] % DH == 0 and width // lax.axis_size("tp") % DH == 0
+    return (kernel_body if aligned else body)(*operands)
+
+
 def solution(mesh):
     return jax.shard_map(
-        body,
+        either_body,
         mesh=mesh,
         in_specs=(
             P("ep", None),

time: 279 us -> 101 us (0.36)
  waiting for transfers between devices: 171 us -> 0 us
  Pallas kernels: 0 us -> 87 us
  blocking collectives: 20.3 us -> 0 us
  matrix products: 18.5 us -> 0 us
  local copies, waits for them, and re-layouts: 26.8 us -> 8.61 us
  between operations: 14.1 us -> 0.71 us
  other arithmetic: 15.7 us -> 4.08 us
  starting transfers between devices: 11.2 us -> 0 us
    pallas_call x0 -> x3, Pallas kernels: none -> 87 us  [the longest x1 39.9 us: mix_and_moe(): pl.pallas_call(functools.partial(moe_kernel, n_ep, n_tp, groups), out_sha...]
    unnamed x5 -> x0, waiting for transfers between devices: 66.2 us -> none
    reduce_scatter x2 -> x0, waiting for transfers between devices: 62.4 us -> none  [the longest x1 49.9 us: body(): lax.psum_scatter(gate_terms, 'ep', scatter_dimension=0, tiled=True)]
    psum x1 -> x0, waiting for transfers between devices: 30.9 us -> none  [body(): lax.psum(partial_mix.astype(jnp.float32).astype(jnp.bfloat16), 'tp')]
    dot_general x8 -> x0, matrix products: 18.5 us -> none  [the longest x1 5.32 us: mlstm_step(): jnp.einsum('bhd,bhde->bhe', queries, memory, precision=lax.Precision.HIGH...]
    all_to_all x1 -> x0, blocking collectives: 14.4 us -> none  [body(): lax.all_to_all(hidden_in, 'ep', split_axis=1, concat_axis=0, tiled=True)]
    all_to_all x2 -> x0, waiting for transfers between devices: 11.8 us -> none  [the longest x1 7.32 us: body(): lax.all_to_all(expert_share, 'ep', split_axis=1, concat_axis=0, tiled=True)]
    all_to_all x2 -> x0, starting transfers between devices: 11 us -> none  [the longest x1 5.53 us: body(): lax.all_to_all(expert_share, 'ep', split_axis=1, concat_axis=0, tiled=True)]
  transfers between devices with their start and end apart: 6 -> 0, of which waited for: 6 -> 0; matrix products, arithmetic and copies ran while one was open for 10% -> 0% of each run, Pallas kernels for 0% -> 0%
where the time goes in v1:
time: 101 us; the launch traced here: 100 us
  Pallas kernels  87 us (86%)
  local copies, waits for them, and re-layouts  8.61 us (9%)
  other arithmetic  4.08 us (4%)
    pallas_call x1, Pallas kernels, mix_and_moe(): pl.pallas_call(functools.partial(moe_kernel, n_ep, n_tp, groups), out_sha...  39.9 us
    pallas_call x1, Pallas kernels, project(): pl.pallas_call(functools.partial(project_kernel, n_ep), out_shape=(jax.Sh...  32.4 us
    pallas_call x1, Pallas kernels, cell(): pl.pallas_call(cell_kernel, grid=(rows,), out_shape=(jax.ShapeDtypeStruct...  14.7 us
    unnamed x11, local copies, waits for them, and re-layouts  5.7 us

profile of v1, /device:TPU:0, one launch (start us, length us, event | category | flops | bytes accessed | tf_op | source)
XLA Modules:
  0.0 100.4 jit_solution(13229873464328721966)
XLA Ops:
  0.6 0.0 copy-start.2
  0.6 0.0 copy-start.1
  0.7 0.0 copy-start
  0.7 0.7 pad_maximum_fusion
  1.4 0.2 copy.33
  1.6 0.7 pad.8.gate_w
  2.3 32.4 %project.1 = (f32[16,2048]{1,0:T(8,128)}, f32[16,128]{1,0:T(8,128)}) custom-call(bf16[16,4096]{1,0:T(8,128)(2,1)} %hidden.3, bf16[512,128]{1,0:T(8,128)(2,1)} %pad.8.gate_w, bf16[512,512]{1,0:T(8,128)(2,1)} %wq.1, bf16[512,512]{1,0:T(8,128)(2,1)} %wk.1, bf16[512,512]{1,0:T(8,128)(2,1)} %wv.1, bf16[512,512]{1,0:T(8,128)(2,1)} %wo.1), custom_call_target="tpu_custom_call" | custom-call | tf_op jit(solution)/shard_map/project/pallas_call | solution.py:284
  34.7 0.8 copy.34
  35.5 0.9 subtract_exponential_fusion
  36.3 0.8 subtract_exponential_fusion.1
  37.2 0.7 broadcast_in_dim.21.keep_ref
  37.9 0.7 broadcast_in_dim.22.write_ref
  38.5 1.6 %copy.37 = f32[2,8,16,128]{3,2,1,0:T(8,128)} copy(f32[2,8,16,128]{3,1,2,0:T(8,128)} %bitcast.24) | data formatting | bytes 262144
  40.1 14.7 %cell.1 = (bf16[16,4,128]{2,1,0:T(4,128)(2,1)}, f32[16,4,16384]{2,1,0:T(4,128)}) custom-call(f32[16,16,128]{2,1,0:T(8,128)} %bitcast.23, f32[16,4,128]{2,1,0:T(4,128)} %broadcast_in_dim.21.keep_ref, f32[16,4,128]{2,1,0:T(4,128)} %broadcast_in_dim.22.write_ref, f32[4,128]{1,0:T(4,128)} %bitcast.29, f32[16,4,16384]{2,1,0:T(4,128)} %mem_ref.1), custom_call_target="tpu_custom_call" | custom-call | tf_op jit(solution)/shard_map/cell/pallas_call | solution.py:332
  54.8 1.3 %copy.40 = bf16[2,8,4,128]{3,1,2,0:T(8,128)(2,1)} copy(bf16[2,8,4,128]{3,2,1,0:T(4,128)(2,1)} %bitcast.27) | data formatting | bytes 32768
  56.1 0.0 copy-done.2
  56.2 0.2 convert_reduce_fusion
  56.4 0.7 fusion.7
  57.0 0.1 select_reduce_fusion
  57.1 0.7 copy.35.route
  57.8 0.0 copy-done.1
  57.8 0.0 copy-done
  57.8 0.7 fusion.3.router_t
  58.5 39.9 %mix_and_moe.1 = bf16[16,1024]{1,0:T(8,128)(2,1)} custom-call(bf16[16,512]{1,0:T(8,128)(2,1)} %bitcast.25, bf16[16,4096]{1,0:T(8,128)(2,1)} %hidden.3, f32[1,4096]{1,0:T(1,128)} %bitcast.26, f32[1,1024]{1,0:T(1,128)} %bitcast.28, bf16[16,4096]{1,0:T(8,128)(2,1)} %fusion.3.router_t, s32[16,2]{1,0:T(8,128)} %copy.35.route, ...), custom_call_target="tpu_custom_call" | custom-call | tf_op jit(solution)/shard_map/mix_and_moe/pallas_call | solution.py:538
  98.4 0.7 copy.36
  99.0 1.4 %copy.42 = bf16[16,1024]{1,0:T(8,128)(2,1)} copy(bf16[16,1024]{1,0:T(8,128)(2,1)} %mix_and_moe.1) | data formatting | bytes 65536
  (3 shorter events, 0.0 us)
Async XLA Ops:
  0.6 55.5 %copy-start.2 = (s32[16,2]{0,1:T(2,128)S(1)}, s32[16,2]{0,1:T(2,128)}, u32[]{:S(2)}) copy-start(s32[16,2]{0,1:T(2,128)} %param.37) | copy-start | bytes 388
  0.6 57.2 %copy-start.1 = (bf16[4096,2]{0,1:T(2,128)(2,1)S(1)}, bf16[4096,2]{0,1:T(2,128)(2,1)}, u32[]{:S(2)}) copy-start(bf16[4096,2]{0,1:T(2,128)(2,1)} %param.35) | copy-start | bytes 49156
  0.7 57.2 %copy-start = (bf16[4096,8]{0,1:T(8,128)(2,1)S(1)}, bf16[4096,8]{0,1:T(8,128)(2,1)}, u32[]{:S(2)}) copy-start(bf16[4096,8]{0,1:T(8,128)(2,1)} %param.36) | copy-start | bytes 196612
